TPU v7x, 32 devices: a whole 2x2x4 slice. The times are simulated.
32 devices in a mesh: kv: 8 (over z, y), tp: 4 (over x, core).
Axes of the slice: x: 2, y: 2, z: 4, core: 2. Of those that a mesh axis runs over, the one named last changes fastest.
Arguments:
- queries: bfloat16 [2048, 3072], P('kv', 'tp'), may hold values from -6 to 6
- key_vectors: bfloat16 [2048, 512], P('kv', 'tp'), may hold values from -6 to 6
- value_vectors: bfloat16 [2048, 512], P('kv', 'tp'), may hold values from -6 to 6
- log_sums: float32 [2048, 48], P('kv', 'tp'), may hold values from 4.5 to 6.5
- out_grad: bfloat16 [2048, 3072], P('kv', 'tp'), may hold values from -48 to 48
- layer_input: bfloat16 [2048, 3072], P('kv', 'tp'), may hold values from -0.29882812 to 0.29882812
- chosen: int32 [32, 16], P('kv'), may hold values from -1 to 55, as said below
Outputs:
- query_grad: bfloat16 [2048, 3072], P('kv', 'tp')
- key_grad: bfloat16 [2048, 512], P('kv', 'tp')
- value_grad: bfloat16 [2048, 512], P('kv', 'tp')
- weight_grad: float32 [3072, 512], P('kv', 'tp')
Inputs may be any that keep to these rules, and one draw needn't show every extreme that they name: `chosen`: each entry is -1 or the number c of a block of 32 positions (c * 32 to c * 32 + 31) that lies wholly within an earlier index of kv than its query block. The numbers of one row differ, and all query blocks held by one index of kv together take at most one block from each other index.
All inputs are finite; a program needn't handle non-finite values.
Results may differ from a plain program's by a relative error of at most 0.0061.
Values may be sent and summed in bfloat16 or wider, within the bound.
No kernel may reach another device: no remote copies, remote signals or barrier semaphores. Data moves between devices by JAX's collectives and lax.ppermute only.
A program may use at most 64 MiB of HBM per device.

v0:
```python
import jax
import jax.numpy as jnp
from jax import lax
from jax.sharding import PartitionSpec as P

HEAD = 64
KB = 32
QB = 64
NSEL = 16


def per_device(queries, key_vectors, value_vectors, log_sums, out_grad, layer_input, chosen):
    axis_count = lax.axis_size("kv")
    own_index = lax.axis_index("kv")
    span_rows = queries.shape[0]
    kv_local = key_vectors.shape[1] // HEAD
    group_size = queries.shape[1] // key_vectors.shape[1]
    blocks_here = span_rows // KB
    query_blocks = span_rows // QB
    score_scale = HEAD ** (-0.5)
    half_width = kv_local * HEAD
    pair_width = 2 * half_width
    paired = jnp.concatenate([key_vectors, value_vectors], axis=1)
    owners = jnp.arange(axis_count, dtype=jnp.int32)
    usable = chosen >= 0
    owner_of = jnp.where(usable, chosen // blocks_here, -1)
    within = chosen - chosen // blocks_here * blocks_here
    matched = owner_of[:, :, None] == owners[None, None, :]
    wanted = jnp.max(jnp.where(matched, within[:, :, None], -1), axis=(0, 1))
    incoming = lax.all_to_all(wanted[:, None], "kv", split_axis=0, concat_axis=0, tiled=True)[:, 0]
    blocks = paired.reshape(blocks_here, KB, pair_width)
    outgoing = jnp.where(
        (incoming >= 0)[:, None, None],
        blocks[jnp.maximum(incoming, 0)],
        jnp.zeros((), paired.dtype),
    )
    fetched = lax.all_to_all(outgoing, "kv", split_axis=0, concat_axis=0, tiled=True)
    query_parts = queries.reshape(query_blocks, QB, kv_local, group_size, HEAD)
    grad_parts = out_grad.reshape(query_blocks, QB, kv_local, group_size, HEAD)
    sum_parts = log_sums.reshape(query_blocks, QB, kv_local, group_size)
    slot_owner = jnp.clip(owner_of, 0, axis_count - 1)
    key_own = key_vectors.reshape(span_rows, kv_local, HEAD)
    value_own = value_vectors.reshape(span_rows, kv_local, HEAD)
    key_pos = own_index * span_rows + jnp.arange(span_rows, dtype=jnp.int32)

    def one_block(packed):
        query_part, grad_part, sum_part, slot_part, usable_part, block_index = packed
        selected = fetched[slot_part].reshape(NSEL * KB, 2, kv_local, HEAD)
        key_sel = selected[:, 0]
        value_sel = selected[:, 1]
        keep_key = jnp.repeat(usable_part, KB)
        query_pos = own_index * span_rows + block_index * QB + jnp.arange(QB, dtype=jnp.int32)
        causal = key_pos[None, :] <= query_pos[:, None]
        score_sel = (
            jnp.einsum("qhgd,khd->qhgk", query_part, key_sel, preferred_element_type=jnp.float32)
            * score_scale
        )
        score_own = (
            jnp.einsum("qhgd,khd->qhgk", query_part, key_own, preferred_element_type=jnp.float32)
            * score_scale
        )
        weight_sel = jnp.where(
            keep_key[None, None, None, :], jnp.exp(score_sel - sum_part[..., None]), 0.0
        )
        weight_own = jnp.where(
            causal[:, None, None, :], jnp.exp(score_own - sum_part[..., None]), 0.0
        )
        round_sel = weight_sel.astype(jnp.bfloat16)
        round_own = weight_own.astype(jnp.bfloat16)
        output = jnp.einsum(
            "qhgk,khd->qhgd", round_sel, value_sel, preferred_element_type=jnp.float32
        )
        output = output + jnp.einsum(
            "qhgk,khd->qhgd", round_own, value_own, preferred_element_type=jnp.float32
        )
        row_delta = jnp.sum(grad_part.astype(jnp.float32) * output, axis=-1)
        prod_sel = jnp.einsum(
            "qhgd,khd->qhgk", grad_part, value_sel, preferred_element_type=jnp.float32
        )
        prod_own = jnp.einsum(
            "qhgd,khd->qhgk", grad_part, value_own, preferred_element_type=jnp.float32
        )
        slope_sel = (weight_sel * (prod_sel - row_delta[..., None])).astype(jnp.bfloat16)
        slope_own = (weight_own * (prod_own - row_delta[..., None])).astype(jnp.bfloat16)
        query_total = jnp.einsum(
            "qhgk,khd->qhgd", slope_sel, key_sel, preferred_element_type=jnp.float32
        )
        query_total = query_total + jnp.einsum(
            "qhgk,khd->qhgd", slope_own, key_own, preferred_element_type=jnp.float32
        )
        query_out = (query_total * score_scale).astype(jnp.bfloat16)
        key_sel_grad = (
            jnp.einsum("qhgk,qhgd->khd", slope_sel, query_part, preferred_element_type=jnp.float32)
            * score_scale
        )
        value_sel_grad = jnp.einsum(
            "qhgk,qhgd->khd", round_sel, grad_part, preferred_element_type=jnp.float32
        )
        key_own_grad = (
            jnp.einsum("qhgk,qhgd->khd", slope_own, query_part, preferred_element_type=jnp.float32)
            * score_scale
        )
        value_own_grad = jnp.einsum(
            "qhgk,qhgd->khd", round_own, grad_part, preferred_element_type=jnp.float32
        )
        sel_pair = jnp.concatenate(
            [
                key_sel_grad.reshape(NSEL, KB, half_width),
                value_sel_grad.reshape(NSEL, KB, half_width),
            ],
            axis=2,
        )
        own_pair = jnp.concatenate(
            [
                key_own_grad.reshape(span_rows, half_width),
                value_own_grad.reshape(span_rows, half_width),
            ],
            axis=1,
        )
        return (query_out, sel_pair, own_pair)

    block_ids = jnp.arange(query_blocks, dtype=jnp.int32)
    query_outs, sel_pairs, own_pairs = lax.map(
        one_block, (query_parts, grad_parts, sum_parts, slot_owner, usable, block_ids)
    )
    onehot = ((slot_owner[:, :, None] == owners[None, None, :]) & usable[:, :, None]).astype(
        jnp.float32
    )
    onehot = onehot.reshape(query_blocks * NSEL, axis_count)
    per_owner = jnp.einsum(
        "so,sr->or",
        onehot,
        sel_pairs.reshape(query_blocks * NSEL, KB * pair_width),
        precision=lax.Precision.HIGHEST,
    )
    returned = lax.all_to_all(
        per_owner.reshape(axis_count, KB, pair_width), "kv", split_axis=0, concat_axis=0, tiled=True
    )
    placing = (incoming[None, :] == jnp.arange(blocks_here, dtype=jnp.int32)[:, None]).astype(
        jnp.float32
    )
    landed = jnp.einsum(
        "bs,sr->br",
        placing,
        returned.reshape(axis_count, KB * pair_width),
        precision=lax.Precision.HIGHEST,
    )
    totals = jnp.sum(own_pairs, axis=0) + landed.reshape(span_rows, pair_width)
    key_grad = totals[:, :half_width].astype(jnp.bfloat16)
    value_grad = totals[:, half_width:].astype(jnp.bfloat16)
    full_input = lax.all_gather(layer_input, "tp", axis=1, tiled=True)
    weight_grad = lax.psum_scatter(
        lax.dot_general(
            full_input, key_grad, (((0,), (0,)), ((), ())), preferred_element_type=jnp.float32
        ),
        "kv",
        scatter_dimension=0,
        tiled=True,
    )
    return (query_outs.reshape(span_rows, queries.shape[1]), key_grad, value_grad, weight_grad)


def solution(mesh):
    placed = (
        P("kv", "tp"),
        P("kv", "tp"),
        P("kv", "tp"),
        P("kv", "tp"),
        P("kv", "tp"),
        P("kv", "tp"),
        P("kv", None),
    )
    return jax.shard_map(
        per_device,
        mesh=mesh,
        in_specs=placed,
        out_specs=(P("kv", "tp"), P("kv", "tp"), P("kv", "tp"), P("kv", "tp")),
        check_vma=False,
    )
```

profile of v0, /device:TPU:0, one launch (start us, length us, event | category | flops | bytes accessed | tf_op | source)
XLA Modules:
  0.0 224.7 jit_solution(12152546866315410712)
XLA Ops:
  9.3 7.3 %all-to-all-start = ((s32[8,1,1]{2,1,0:T(1,128)}), s32[8,1,1]{2,1,0:T(1,128)S(1)}, u32[]{:S(2)}, u32[]{:S(2)}) async-start(s32[8,1,1]{2,1,0:T(1,128)} %copy.110), calls=%async_computation | async-start | bytes 8192 | tf_op jit(solution)/shard_map/all_to_all | solution.py:30
  17.5 5.5 %all-to-all-done = s32[8,1,1]{2,1,0:T(1,128)S(1)} async-done(((s32[8,1,1]{2,1,0:T(1,128)}), s32[8,1,1]{2,1,0:T(1,128)S(1)}, u32[]{:S(2)}, u32[]{:S(2)}) %all-to-all-start) | async-done | bytes 64 | tf_op jit(solution)/shard_map/all_to_all | solution.py:30
  24.9 3.4 %all-to-all-start.1 = ((bf16[8,32,256]{2,1,0:T(8,128)(2,1)}), bf16[8,32,256]{2,1,0:T(8,128)(2,1)S(1)}, u32[]{:S(2)}, u32[]{:S(2)}) async-start(bf16[8,32,256]{2,1,0:T(8,128)(2,1)} %broadcast_select_fusion), calls=%async_computation.1 | async-start | bytes 262144 | tf_op jit(solution)/shard_map/all_to_all | solution.py:37
  29.1 1.6 copy.113
  36.9 93.2 %while.18 = (s32[]{:T(128)}, bf16[4,64,2,6,64]{1,4,3,2,0:T(8,128)(2,1)}, f32[4,16,32,256]{3,2,1,0:T(8,128)}, f32[4,256,256]{1,2,0:T(8,128)}, s32[4,16]{1,0:T(4,1...) while((s32[]{:T(128)}, ...), condition=%wide.region_3.4_spmd.clone.clone, body=%wide.region_1.3_spmd.clone.clone.sunk | while | flops 458359424 | bytes 25241412 | solution.py:123
  39.2 1.4 fusion.153
  48.6 2.0 reshape.226
  58.5 1.8 fusion.158
  62.5 1.4 fusion.153
  71.9 2.0 reshape.226
  81.7 1.8 fusion.158
  85.8 1.4 fusion.153
  95.1 2.0 reshape.226
  105.0 1.8 fusion.158
  109.1 1.4 fusion.153
  118.4 2.0 reshape.226
  128.3 1.8 fusion.158
  130.1 3.5 %fusion.66 = f32[8,32,256]{2,0,1:T(8,128)S(1)} fusion(s32[64]{0:T(128)} %eq.51, pred[64]{0:T(512)(128)(4,1)} %and.19, f32[8,8,32,256]{3,2,1,0:T(8,128)} %bitcast.274), kind=kOutput, calls=%fused_computation.90 | convolution fusion | flops 50332672 | bytes 2359616 | tf_op jit(solution)/shard_map/so,sr->or/dot_general | solution.py:130
  134.5 5.9 %all-to-all-start.2 = ((f32[8,32,256]{2,1,0:T(8,128)}), f32[8,32,256]{2,1,0:T(8,128)S(1)}, u32[]{:S(2)}, u32[]{:S(2)}) async-start(f32[8,32,256]{2,1,0:T(8,128)} %copy.120), calls=%async_computation.2 | async-start | bytes 524288 | tf_op jit(solution)/shard_map/all_to_all | solution.py:136
  140.7 7.9 %all-to-all-done.2 = f32[8,32,256]{2,1,0:T(8,128)S(1)} async-done(((f32[8,32,256]{2,1,0:T(8,128)}), f32[8,32,256]{2,1,0:T(8,128)S(1)}, u32[]{:S(2)}, u32[]{:S(2)}) %all-to-all-start.2) | async-done | bytes 262176 | tf_op jit(solution)/shard_map/all_to_all | solution.py:136
  149.3 2.9 %convolution_bitcast_fusion.8 = f32[3072,128]{0,1:T(8,128)} fusion(bf16[256,3072]{1,0:T(8,128)(2,1)} %all-gather.2.cloned.1.call-done, bf16[256,256]{0,1:T(8,128)(2,1)S(1)} %add_convert_fusion), kind=kOutput, calls=%fused_computation.89 | convolution fusion | flops 201326592 | bytes 3211264 | tf_op jit(solution)/shard_map/dot_general | solution.py:153
  154.3 1.4 reshape.213
  157.2 58.9 %reduce-scatter.2.cloned.1.call-done = f32[384,128]{0,1:T(8,128)} async-done(((f32[3072,128]{0,1:T(8,128)}), f32[384,128]{0,1:T(8,128)}) %reduce-scatter.2.cloned.1.call-update) | async-done | bytes 196624 | tf_op jit(solution)/shard_map/reduce_scatter | solution.py:152
  216.1 1.7 copy.125
  (230 shorter events, 85.8 us)
Async XLA Ops:
  7.2 23.5 %copy-start.7 = (bf16[256,128]{1,0:T(8,128)(2,1)S(1)}, bf16[256,128]{1,0:T(8,128)(2,1)}, u32[]{:S(2)}) copy-start(bf16[256,128]{1,0:T(8,128)(2,1)} %param.11) | copy-start | bytes 196612
  7.2 24.2 %copy-start.5 = (bf16[256,768]{1,0:T(8,128)(2,1)S(1)}, bf16[256,768]{1,0:T(8,128)(2,1)}, u32[]{:S(2)}) copy-start(bf16[256,768]{1,0:T(8,128)(2,1)} %param.9) | copy-start | bytes 1179652
  9.3 13.7 %all-to-all-start = ((s32[8,1,1]{2,1,0:T(1,128)}), s32[8,1,1]{2,1,0:T(1,128)S(1)}, u32[]{:S(2)}, u32[]{:S(2)}) async-start(s32[8,1,1]{2,1,0:T(1,128)} %copy.110), calls=%async_computation | async-start | bytes 8192 | tf_op jit(solution)/shard_map/all_to_all | solution.py:30
  24.9 12.0 %all-to-all-start.1 = ((bf16[8,32,256]{2,1,0:T(8,128)(2,1)}), bf16[8,32,256]{2,1,0:T(8,128)(2,1)S(1)}, u32[]{:S(2)}, u32[]{:S(2)}) async-start(bf16[8,32,256]{2,1,0:T(8,128)(2,1)} %broadcast_select_fusion), calls=%async_computation.1 | async-start | bytes 262144 | tf_op jit(solution)/shard_map/all_to_all | solution.py:37
  28.3 120.9 %all-gather.2.cloned.1.call-start = ((), (), s32[]{:S(2)}) async-start(), calls=%async_computation.4 | async-start | bytes 1966080 | tf_op jit(solution)/shard_map/all_gather | solution.py:151
  36.9 4.2 %copy-start.11 = (s32[4]{0:T(128)}, s32[4]{0:T(128)S(1)}, u32[]{:S(2)}) copy-start(s32[4]{0:T(128)S(1)} %get-tuple-element.490) | copy-start | bytes 52 | tf_op jit(solution)/shard_map/while
  53.6 4.3 %copy-start.2 = (bf16[512,1,2,64]{0,3,2,1:T(8,128)(2,1)S(1)}, bf16[512,1,2,64]{0,3,2,1:T(8,128)(2,1)}, u32[]{:S(2)}) copy-start(bf16[512,1,2,64]{0,3,2,1:T(8,128)(2,1)} %copy-done.1) | copy-start | bytes 393220 | tf_op jit(solution)/shard_map/while
  57.2 3.1 %copy-start.9 = (f32[4,64,2,6]{1,0,3,2:T(4,128)S(1)}, f32[4,64,2,6]{1,0,3,2:T(4,128)}, u32[]{:S(2)}) copy-start(f32[4,64,2,6]{1,0,3,2:T(4,128)} %copy-done.8) | copy-start | bytes 36868 | tf_op jit(solution)/shard_map/while
  57.2 3.1 %copy-start.12 = (s32[4]{0:T(128)S(1)}, s32[4]{0:T(128)}, u32[]{:S(2)}) copy-start(s32[4]{0:T(128)} %copy-done.11) | copy-start | bytes 52 | tf_op jit(solution)/shard_map/while
  60.3 4.1 %copy-start.11 = (s32[4]{0:T(128)}, s32[4]{0:T(128)S(1)}, u32[]{:S(2)}) copy-start(s32[4]{0:T(128)S(1)} %get-tuple-element.490) | copy-start | bytes 52 | tf_op jit(solution)/shard_map/while
  76.9 4.3 %copy-start.2 = (bf16[512,1,2,64]{0,3,2,1:T(8,128)(2,1)S(1)}, bf16[512,1,2,64]{0,3,2,1:T(8,128)(2,1)}, u32[]{:S(2)}) copy-start(bf16[512,1,2,64]{0,3,2,1:T(8,128)(2,1)} %copy-done.1) | copy-start | bytes 393220 | tf_op jit(solution)/shard_map/while
  80.5 3.1 %copy-start.9 = (f32[4,64,2,6]{1,0,3,2:T(4,128)S(1)}, f32[4,64,2,6]{1,0,3,2:T(4,128)}, u32[]{:S(2)}) copy-start(f32[4,64,2,6]{1,0,3,2:T(4,128)} %copy-done.8) | copy-start | bytes 36868 | tf_op jit(solution)/shard_map/while
  80.5 3.1 %copy-start.12 = (s32[4]{0:T(128)S(1)}, s32[4]{0:T(128)}, u32[]{:S(2)}) copy-start(s32[4]{0:T(128)} %copy-done.11) | copy-start | bytes 52 | tf_op jit(solution)/shard_map/while
  83.5 4.1 %copy-start.11 = (s32[4]{0:T(128)}, s32[4]{0:T(128)S(1)}, u32[]{:S(2)}) copy-start(s32[4]{0:T(128)S(1)} %get-tuple-element.490) | copy-start | bytes 52 | tf_op jit(solution)/shard_map/while
  100.2 4.3 %copy-start.2 = (bf16[512,1,2,64]{0,3,2,1:T(8,128)(2,1)S(1)}, bf16[512,1,2,64]{0,3,2,1:T(8,128)(2,1)}, u32[]{:S(2)}) copy-start(bf16[512,1,2,64]{0,3,2,1:T(8,128)(2,1)} %copy-done.1) | copy-start | bytes 393220 | tf_op jit(solution)/shard_map/while
  103.8 3.1 %copy-start.9 = (f32[4,64,2,6]{1,0,3,2:T(4,128)S(1)}, f32[4,64,2,6]{1,0,3,2:T(4,128)}, u32[]{:S(2)}) copy-start(f32[4,64,2,6]{1,0,3,2:T(4,128)} %copy-done.8) | copy-start | bytes 36868 | tf_op jit(solution)/shard_map/while
  103.8 3.1 %copy-start.12 = (s32[4]{0:T(128)S(1)}, s32[4]{0:T(128)}, u32[]{:S(2)}) copy-start(s32[4]{0:T(128)} %copy-done.11) | copy-start | bytes 52 | tf_op jit(solution)/shard_map/while
  106.9 4.1 %copy-start.11 = (s32[4]{0:T(128)}, s32[4]{0:T(128)S(1)}, u32[]{:S(2)}) copy-start(s32[4]{0:T(128)S(1)} %get-tuple-element.490) | copy-start | bytes 52 | tf_op jit(solution)/shard_map/while
  123.5 4.3 %copy-start.2 = (bf16[512,1,2,64]{0,3,2,1:T(8,128)(2,1)S(1)}, bf16[512,1,2,64]{0,3,2,1:T(8,128)(2,1)}, u32[]{:S(2)}) copy-start(bf16[512,1,2,64]{0,3,2,1:T(8,128)(2,1)} %copy-done.1) | copy-start | bytes 393220 | tf_op jit(solution)/shard_map/while
  127.0 3.1 %copy-start.9 = (f32[4,64,2,6]{1,0,3,2:T(4,128)S(1)}, f32[4,64,2,6]{1,0,3,2:T(4,128)}, u32[]{:S(2)}) copy-start(f32[4,64,2,6]{1,0,3,2:T(4,128)} %copy-done.8) | copy-start | bytes 36868 | tf_op jit(solution)/shard_map/while
  127.0 3.1 %copy-start.12 = (s32[4]{0:T(128)S(1)}, s32[4]{0:T(128)}, u32[]{:S(2)}) copy-start(s32[4]{0:T(128)} %copy-done.11) | copy-start | bytes 52 | tf_op jit(solution)/shard_map/while
  130.1 10.5 %copy-start.3 = (f32[4,256,256]{1,2,0:T(8,128)S(1)}, f32[4,256,256]{1,2,0:T(8,128)}, u32[]{:S(2)}) copy-start(f32[4,256,256]{1,2,0:T(8,128)} %get-tuple-element.178) | copy-start | bytes 3145732
  134.5 14.1 %all-to-all-start.2 = ((f32[8,32,256]{2,1,0:T(8,128)}), f32[8,32,256]{2,1,0:T(8,128)S(1)}, u32[]{:S(2)}, u32[]{:S(2)}) async-start(f32[8,32,256]{2,1,0:T(8,128)} %copy.120), calls=%async_computation.2 | async-start | bytes 524288 | tf_op jit(solution)/shard_map/all_to_all | solution.py:136
  140.4 75.8 %reduce-scatter.2.cloned.1.call-start = ((), (), s32[]{:S(2)}) async-start(), calls=%async_computation.5 | async-start | bytes 1769472 | tf_op jit(solution)/shard_map/reduce_scatter | solution.py:152
  (15 other events, 26.6 us)
Sparse Core Ops, SparseCore 0:
  30.7 20.9 all-gather.1
  152.3 63.7 reduce-scatter.1
where the time goes:
time: 227 us; the launch traced here: 225 us
  waiting for transfers between devices  73.1 us (32%)
  matrix products  62.1 us (27%)
  local copies, waits for them, and re-layouts  44.4 us (20%)
  starting transfers between devices  16.9 us (7%)
  between operations  14.2 us (6%)
  other arithmetic  10.4 us (5%)
  loops' own time  3.57 us (2%)
    reduce_scatter x1, waiting for transfers between devices, per_device(): lax.psum_scatter(lax.dot_general(full_input, key_grad, (((0,), (0,)), (()...  58.9 us
    unnamed x22, local copies, waits for them, and re-layouts  11.4 us
    reshape x4, local copies, waits for them, and re-layouts, one_block(): key_sel_grad.reshape(NSEL, KB, half_width)  8.17 us
    all_to_all x1, waiting for transfers between devices, per_device(): lax.all_to_all(per_owner.reshape(axis_count, KB, pair_width), 'kv', split...  7.9 us
    dot_general x4, matrix products, one_block(): jnp.einsum('qhgk,khd->qhgd', slope_own, key_own, preferred_element_type=j...  7.34 us
    all_to_all x1, starting transfers between devices, per_device(): lax.all_to_all(wanted[:, None], 'kv', split_axis=0, concat_axis=0, tiled=...  7.31 us
    dynamic_update_slice x8, other arithmetic, per_device(): lax.map(one_block, (query_parts, grad_parts, sum_parts, slot_owner, usabl...  6.22 us
    all_to_all x1, starting transfers between devices, per_device(): lax.all_to_all(per_owner.reshape(axis_count, KB, pair_width), 'kv', split...  5.91 us
  transfers between devices with their start and end apart: 5, of which 3 were waited for; matrix products, arithmetic and copies ran while one was open for 47% of the time, Pallas kernels for 0%

commit v1 on v0

--- a/solution.py
+++ b/solution.py
@@ -7,6 +7,29 @@
 KB = 32
 QB = 64
 NSEL = 16
+
+
+def in_blocks(x, dim, size):
+    lengths = x.shape
+    blocks = x.reshape(*lengths[:dim], size, lengths[dim] // size, *lengths[dim + 1 :])
+    return jnp.moveaxis(blocks, dim, 0)
+
+
+def joined_along(blocks, dim):
+    blocks = jnp.moveaxis(blocks, 0, dim)
+    shape = blocks.shape
+    return blocks.reshape(*shape[:dim], shape[dim] * shape[dim + 1], *shape[dim + 2 :])
+
+
+def rotated_exchange(x, axis, split_dim, concat_dim):
+    size, position = (lax.axis_size(axis), lax.axis_index(axis))
+    blocks = in_blocks(x, split_dim, size)
+    outs = [blocks[position]]
+    for turn in range(1, size):
+        sent = blocks[(position + turn) % size]
+        outs.append(lax.ppermute(sent, axis, [(i, (i + turn) % size) for i in range(size)]))
+    blocks = jnp.stack(outs)[(position - jnp.arange(size)) % size]
+    return joined_along(blocks, concat_dim)
 
 
 def per_device(queries, key_vectors, value_vectors, log_sums, out_grad, layer_input, chosen):
@@ -27,7 +50,7 @@
     within = chosen - chosen // blocks_here * blocks_here
     matched = owner_of[:, :, None] == owners[None, None, :]
     wanted = jnp.max(jnp.where(matched, within[:, :, None], -1), axis=(0, 1))
-    incoming = lax.all_to_all(wanted[:, None], "kv", split_axis=0, concat_axis=0, tiled=True)[:, 0]
+    incoming = rotated_exchange(wanted[:, None], "kv", 0, 0)[:, 0]
     blocks = paired.reshape(blocks_here, KB, pair_width)
     outgoing = jnp.where(
         (incoming >= 0)[:, None, None],

time: 227 us -> 236 us (1.040)
  starting transfers between devices: 16.9 us -> 25.1 us
  local copies, waits for them, and re-layouts: 44.4 us -> 49.7 us
  waiting for transfers between devices: 73.1 us -> 69.6 us
    ppermute x0 -> x7, starting transfers between devices: none -> 13.8 us  [rotated_exchange(): lax.ppermute(sent, axis, [(i, (i + turn) % size) for i in range(size)])]
    all_to_all x1 -> x0, starting transfers between devices: 7.31 us -> none  [per_device(): lax.all_to_all(wanted[:, None], 'kv', split_axis=0, concat_axis=0, tiled=...]
    all_to_all x1 -> x0, waiting for transfers between devices: 5.53 us -> none  [per_device(): lax.all_to_all(wanted[:, None], 'kv', split_axis=0, concat_axis=0, tiled=...]
    another operation x0 -> x1, local copies, waits for them, and re-layouts: none -> 5.27 us  [rotated_exchange(): blocks = jnp.stack(outs)[(position - jnp.arange(size)) % size]]
    unnamed x22 -> x24, local copies, waits for them, and re-layouts: 11.4 us -> 10.5 us
  transfers between devices with their start and end apart: 5 -> 11, of which waited for: 3 -> 4; matrix products, arithmetic and copies ran while one was open for 47% -> 45% of each run, Pallas kernels for 0% -> 0%
where the time goes in v1:
time: 236 us; the launch traced here: 234 us
  waiting for transfers between devices  69.6 us (29%)
  matrix products  62.2 us (26%)
  local copies, waits for them, and re-layouts  49.7 us (21%)
  starting transfers between devices  25.1 us (11%)
  between operations  14.3 us (6%)
  other arithmetic  9.91 us (4%)
  loops' own time  3.57 us (2%)
    reduce_scatter x1, waiting for transfers between devices, per_device(): lax.psum_scatter(lax.dot_general(full_input, key_grad, (((0,), (0,)), (()...  59.2 us
    ppermute x7, starting transfers between devices, rotated_exchange(): lax.ppermute(sent, axis, [(i, (i + turn) % size) for i in range(size)])  13.8 us
    unnamed x24, local copies, waits for them, and re-layouts  10.5 us
    reshape x4, local copies, waits for them, and re-layouts, one_block(): key_sel_grad.reshape(NSEL, KB, half_width)  8.19 us
    all_to_all x1, waiting for transfers between devices, per_device(): lax.all_to_all(per_owner.reshape(axis_count, KB, pair_width), 'kv', split...  7.9 us
    dot_general x4, matrix products, one_block(): jnp.einsum('qhgk,khd->qhgd', slope_own, key_own, preferred_element_type=j...  7.41 us
    dynamic_update_slice x8, other arithmetic, per_device(): lax.map(one_block, (query_parts, grad_parts, sum_parts, slot_owner, usabl...  6.28 us
    all_to_all x1, starting transfers between devices, per_device(): lax.all_to_all(per_owner.reshape(axis_count, KB, pair_width), 'kv', split...  5.95 us
  transfers between devices with their start and end apart: 11, of which 4 were waited for; matrix products, arithmetic and copies ran while one was open for 45% of the time, Pallas kernels for 0%

profile of v1, /device:TPU:0, one launch (start us, length us, event | category | flops | bytes accessed | tf_op | source)
XLA Modules:
  0.0 234.4 jit_solution(4898858602396066675)
XLA Ops:
  9.4 5.0 %collective-permute-start.4 = (s32[1,1]{1,0:T(1,128)}, s32[1,1]{1,0:T(1,128)}, u32[]{:S(2)}, u32[]{:S(2)}) collective-permute-start(s32[1,1]{1,0:T(1,128)} %bitcast.9), channel_id=1, source_target_pairs={{0,20},{4,24},{8,28},{12,0},{16,4},{20,8},{24,12},{28,16},{1,21},{... | collective-permute-start | bytes 20 | tf_op jit(solution)/shard_map/ppermute | solution.py:30
  16.3 1.5 collective-permute-start
  19.4 1.9 collective-permute-start.2
  21.3 2.8 %collective-permute-start.3 = (s32[1,1]{1,0:T(1,128)}, s32[1,1]{1,0:T(1,128)}, u32[]{:S(2)}, u32[]{:S(2)}) collective-permute-start(s32[1,1]{1,0:T(1,128)} %bitcast.7), channel_id=1, source_target_pairs={{0,16},{4,20},{8,24},{12,28},{16,0},{20,4},{24,8},{28,12},{1,17},{... | collective-permute-start | bytes 20 | tf_op jit(solution)/shard_map/ppermute | solution.py:30
  25.9 5.3 %stack.31 = s32[8,1,1]{0,2,1:T(1,128)S(1)} concatenate(s32[1,1,1]{0,2,1:T(1,128)} %bitcast, s32[1,1,1]{0,2,1:T(1,128)} %bitcast.2, s32[1,1,1]{0,2,1:T(1,128)} %bitcast.4, s32[1,1,1]{0,2,1:T(1,128)} %bitcast.6, s32[1,1,1]{0,2,1:T(1,128)} %bitcast.8, s32[1,1,1]{0,2,1:T(1,128)} %bitcast.10, s32[1,1,1]{0,2,1:T(1,128)} %bitcast.12, s32[1,1,1]{0,2,1:T(1,128)} %bitcast.14), dimensions={0} | concatenate | bytes 64 | tf_op jit(solution)/shard_map/stack | solution.py:31
  33.1 5.1 %all-to-all-start = ((bf16[8,32,256]{2,1,0:T(8,128)(2,1)}), bf16[8,32,256]{2,1,0:T(8,128)(2,1)S(1)}, u32[]{:S(2)}, u32[]{:S(2)}) async-start(bf16[8,32,256]{2,1,0:T(8,128)(2,1)} %broadcast_select_fusion), calls=%async_computation | async-start | bytes 262144 | tf_op jit(solution)/shard_map/all_to_all | solution.py:60
  46.1 93.4 %while.18 = (s32[]{:T(128)}, bf16[4,64,2,6,64]{1,4,3,2,0:T(8,128)(2,1)}, f32[4,16,32,256]{3,2,1,0:T(8,128)}, f32[4,256,256]{1,2,0:T(8,128)}, s32[4,16]{1,0:T(4,1...) while((s32[]{:T(128)}, ...), condition=%wide.region_3.4_spmd.clone.clone, body=%wide.region_1.3_spmd.clone.clone.sunk | while | flops 458359424 | bytes 25241412 | solution.py:146
  48.4 1.4 fusion.155
  57.7 2.1 reshape.303
  67.6 1.8 fusion.160
  81.1 2.0 reshape.303
  90.9 1.9 fusion.160
  104.4 2.0 reshape.303
  114.3 1.9 fusion.160
  118.4 1.4 fusion.155
  127.7 2.0 reshape.303
  137.6 1.8 fusion.160
  139.5 3.5 %fusion.66 = f32[8,32,256]{2,0,1:T(8,128)S(1)} fusion(s32[64]{0:T(128)} %eq.58, pred[64]{0:T(512)(128)(4,1)} %and.74, f32[8,8,32,256]{3,2,1,0:T(8,128)} %bitcast.292), kind=kOutput, calls=%fused_computation.91 | convolution fusion | flops 50332672 | bytes 2359616 | tf_op jit(solution)/shard_map/so,sr->or/dot_general | solution.py:153
  143.8 6.0 %all-to-all-start.1 = ((f32[8,32,256]{2,1,0:T(8,128)}), f32[8,32,256]{2,1,0:T(8,128)S(1)}, u32[]{:S(2)}, u32[]{:S(2)}) async-start(f32[8,32,256]{2,1,0:T(8,128)} %copy.91), calls=%async_computation.1 | async-start | bytes 524288 | tf_op jit(solution)/shard_map/all_to_all | solution.py:159
  150.1 7.9 %all-to-all-done.1 = f32[8,32,256]{2,1,0:T(8,128)S(1)} async-done(((f32[8,32,256]{2,1,0:T(8,128)}), f32[8,32,256]{2,1,0:T(8,128)S(1)}, u32[]{:S(2)}, u32[]{:S(2)}) %all-to-all-start.1) | async-done | bytes 262176 | tf_op jit(solution)/shard_map/all_to_all | solution.py:159
  158.7 2.9 %convolution_bitcast_fusion.8 = f32[3072,128]{0,1:T(8,128)} fusion(bf16[256,3072]{1,0:T(8,128)(2,1)} %all-gather.2.cloned.1.call-done, bf16[256,256]{0,1:T(8,128)(2,1)S(1)} %add_convert_fusion), kind=kOutput, calls=%fused_computation.90 | convolution fusion | flops 201326592 | bytes 3211264 | tf_op jit(solution)/shard_map/dot_general | solution.py:176
  163.7 1.4 reshape.293
  166.6 59.2 %reduce-scatter.2.cloned.1.call-done = f32[384,128]{0,1:T(8,128)} async-done(((f32[3072,128]{0,1:T(8,128)}), f32[384,128]{0,1:T(8,128)}) %reduce-scatter.2.cloned.1.call-update) | async-done | bytes 196624 | tf_op jit(solution)/shard_map/reduce_scatter | solution.py:175
  225.8 1.7 copy.96
  (248 shorter events, 93.8 us)
Async XLA Ops:
  7.2 31.8 %copy-start.7 = (bf16[256,128]{1,0:T(8,128)(2,1)S(1)}, bf16[256,128]{1,0:T(8,128)(2,1)}, u32[]{:S(2)}) copy-start(bf16[256,128]{1,0:T(8,128)(2,1)} %param.10) | copy-start | bytes 196612
  7.2 32.6 %copy-start.8 = (bf16[256,128]{1,0:T(8,128)(2,1)S(1)}, bf16[256,128]{1,0:T(8,128)(2,1)}, u32[]{:S(2)}) copy-start(bf16[256,128]{1,0:T(8,128)(2,1)} %param.11) | copy-start | bytes 196612
  7.2 33.3 %copy-start.5 = (bf16[256,768]{1,0:T(8,128)(2,1)S(1)}, bf16[256,768]{1,0:T(8,128)(2,1)}, u32[]{:S(2)}) copy-start(bf16[256,768]{1,0:T(8,128)(2,1)} %param.9) | copy-start | bytes 1179652
  9.4 10.0 %collective-permute-start.4 = (s32[1,1]{1,0:T(1,128)}, s32[1,1]{1,0:T(1,128)}, u32[]{:S(2)}, u32[]{:S(2)}) collective-permute-start(s32[1,1]{1,0:T(1,128)} %bitcast.9), channel_id=1, source_target_pairs={{0,20},{4,24},{8,28},{12,0},{16,4},{20,8},{24,12},{28,16},{1,21},{... | collective-permute-start | bytes 20 | tf_op jit(solution)/shard_map/ppermute | solution.py:30
  14.4 6.9 %collective-permute-start.5 = (s32[1,1]{1,0:T(1,128)}, s32[1,1]{1,0:T(1,128)}, u32[]{:S(2)}, u32[]{:S(2)}) collective-permute-start(s32[1,1]{1,0:T(1,128)} %bitcast.11), channel_id=1, source_target_pairs={{0,24},{4,28},{8,0},{12,4},{16,8},{20,12},{24,16},{28,20},{1,25},{... | collective-permute-start | bytes 20 | tf_op jit(solution)/shard_map/ppermute | solution.py:30
  15.8 8.4 %collective-permute-start.6 = (s32[1,1]{1,0:T(1,128)}, s32[1,1]{1,0:T(1,128)}, u32[]{:S(2)}, u32[]{:S(2)}) collective-permute-start(s32[1,1]{1,0:T(1,128)} %bitcast.13), channel_id=1, source_target_pairs={{0,28},{4,0},{8,4},{12,8},{16,12},{20,16},{24,20},{28,24},{1,29},{... | collective-permute-start | bytes 20 | tf_op jit(solution)/shard_map/ppermute | solution.py:30
  16.3 7.9 %collective-permute-start = (s32[1,1]{1,0:T(1,128)}, s32[1,1]{1,0:T(1,128)}, u32[]{:S(2)}, u32[]{:S(2)}) collective-permute-start(s32[1,1]{1,0:T(1,128)} %bitcast.1), channel_id=1, source_target_pairs={{0,4},{4,8},{8,12},{12,16},{16,20},{20,24},{24,28},{28,0},{1,5},{5... | collective-permute-start | bytes 20 | tf_op jit(solution)/shard_map/ppermute | solution.py:30
  17.8 6.3 %collective-permute-start.1 = (s32[1,1]{1,0:T(1,128)}, s32[1,1]{1,0:T(1,128)}, u32[]{:S(2)}, u32[]{:S(2)}) collective-permute-start(s32[1,1]{1,0:T(1,128)} %bitcast.3), channel_id=1, source_target_pairs={{0,8},{4,12},{8,16},{12,20},{16,24},{20,28},{24,0},{28,4},{1,9},{5... | collective-permute-start | bytes 20 | tf_op jit(solution)/shard_map/ppermute | solution.py:30
  19.4 5.4 %collective-permute-start.2 = (s32[1,1]{1,0:T(1,128)}, s32[1,1]{1,0:T(1,128)}, u32[]{:S(2)}, u32[]{:S(2)}) collective-permute-start(s32[1,1]{1,0:T(1,128)} %bitcast.5), channel_id=1, source_target_pairs={{0,12},{4,16},{8,20},{12,24},{16,28},{20,0},{24,4},{28,8},{1,13},{... | collective-permute-start | bytes 20 | tf_op jit(solution)/shard_map/ppermute | solution.py:30
  21.3 4.6 %collective-permute-start.3 = (s32[1,1]{1,0:T(1,128)}, s32[1,1]{1,0:T(1,128)}, u32[]{:S(2)}, u32[]{:S(2)}) collective-permute-start(s32[1,1]{1,0:T(1,128)} %bitcast.7), channel_id=1, source_target_pairs={{0,16},{4,20},{8,24},{12,28},{16,0},{20,4},{24,8},{28,12},{1,17},{... | collective-permute-start | bytes 20 | tf_op jit(solution)/shard_map/ppermute | solution.py:30
  33.1 13.0 %all-to-all-start = ((bf16[8,32,256]{2,1,0:T(8,128)(2,1)}), bf16[8,32,256]{2,1,0:T(8,128)(2,1)S(1)}, u32[]{:S(2)}, u32[]{:S(2)}) async-start(bf16[8,32,256]{2,1,0:T(8,128)(2,1)} %broadcast_select_fusion), calls=%async_computation | async-start | bytes 262144 | tf_op jit(solution)/shard_map/all_to_all | solution.py:60
  38.2 120.4 %all-gather.2.cloned.1.call-start = ((), (), s32[]{:S(2)}) async-start(), calls=%async_computation.3 | async-start | bytes 1966080 | tf_op jit(solution)/shard_map/all_gather | solution.py:174
  46.1 4.2 %copy-start.12 = (s32[4]{0:T(128)}, s32[4]{0:T(128)S(1)}, u32[]{:S(2)}) copy-start(s32[4]{0:T(128)S(1)} %get-tuple-element.478) | copy-start | bytes 52 | tf_op jit(solution)/shard_map/while
  62.8 4.3 %copy-start.2 = (bf16[512,1,2,64]{0,3,2,1:T(8,128)(2,1)S(1)}, bf16[512,1,2,64]{0,3,2,1:T(8,128)(2,1)}, u32[]{:S(2)}) copy-start(bf16[512,1,2,64]{0,3,2,1:T(8,128)(2,1)} %copy-done.1) | copy-start | bytes 393220 | tf_op jit(solution)/shard_map/while
  69.5 4.2 %copy-start.12 = (s32[4]{0:T(128)}, s32[4]{0:T(128)S(1)}, u32[]{:S(2)}) copy-start(s32[4]{0:T(128)S(1)} %get-tuple-element.478) | copy-start | bytes 52 | tf_op jit(solution)/shard_map/while
  86.1 4.3 %copy-start.2 = (bf16[512,1,2,64]{0,3,2,1:T(8,128)(2,1)S(1)}, bf16[512,1,2,64]{0,3,2,1:T(8,128)(2,1)}, u32[]{:S(2)}) copy-start(bf16[512,1,2,64]{0,3,2,1:T(8,128)(2,1)} %copy-done.1) | copy-start | bytes 393220 | tf_op jit(solution)/shard_map/while
  92.8 4.2 %copy-start.12 = (s32[4]{0:T(128)}, s32[4]{0:T(128)S(1)}, u32[]{:S(2)}) copy-start(s32[4]{0:T(128)S(1)} %get-tuple-element.478) | copy-start | bytes 52 | tf_op jit(solution)/shard_map/while
  109.4 4.3 %copy-start.2 = (bf16[512,1,2,64]{0,3,2,1:T(8,128)(2,1)S(1)}, bf16[512,1,2,64]{0,3,2,1:T(8,128)(2,1)}, u32[]{:S(2)}) copy-start(bf16[512,1,2,64]{0,3,2,1:T(8,128)(2,1)} %copy-done.1) | copy-start | bytes 393220 | tf_op jit(solution)/shard_map/while
  113.0 3.1 %copy-start.10 = (f32[4,64,2,6]{1,0,3,2:T(4,128)S(1)}, f32[4,64,2,6]{1,0,3,2:T(4,128)}, u32[]{:S(2)}) copy-start(f32[4,64,2,6]{1,0,3,2:T(4,128)} %copy-done.9) | copy-start | bytes 36868 | tf_op jit(solution)/shard_map/while
  116.1 4.2 %copy-start.12 = (s32[4]{0:T(128)}, s32[4]{0:T(128)S(1)}, u32[]{:S(2)}) copy-start(s32[4]{0:T(128)S(1)} %get-tuple-element.478) | copy-start | bytes 52 | tf_op jit(solution)/shard_map/while
  132.8 4.3 %copy-start.2 = (bf16[512,1,2,64]{0,3,2,1:T(8,128)(2,1)S(1)}, bf16[512,1,2,64]{0,3,2,1:T(8,128)(2,1)}, u32[]{:S(2)}) copy-start(bf16[512,1,2,64]{0,3,2,1:T(8,128)(2,1)} %copy-done.1) | copy-start | bytes 393220 | tf_op jit(solution)/shard_map/while
  139.5 10.5 %copy-start.3 = (f32[4,256,256]{1,2,0:T(8,128)S(1)}, f32[4,256,256]{1,2,0:T(8,128)}, u32[]{:S(2)}) copy-start(f32[4,256,256]{1,2,0:T(8,128)} %get-tuple-element.178) | copy-start | bytes 3145732
  143.8 14.2 %all-to-all-start.1 = ((f32[8,32,256]{2,1,0:T(8,128)}), f32[8,32,256]{2,1,0:T(8,128)S(1)}, u32[]{:S(2)}, u32[]{:S(2)}) async-start(f32[8,32,256]{2,1,0:T(8,128)} %copy.91), calls=%async_computation.1 | async-start | bytes 524288 | tf_op jit(solution)/shard_map/all_to_all | solution.py:159
  149.8 76.0 %reduce-scatter.2.cloned.1.call-start = ((), (), s32[]{:S(2)}) async-start(), calls=%async_computation.4 | async-start | bytes 1769472 | tf_op jit(solution)/shard_map/reduce_scatter | solution.py:175
  (22 other events, 48.5 us)
Sparse Core Ops, SparseCore 0:
  40.6 21.0 all-gather.1
  161.8 64.0 reduce-scatter.1
